TPU v7x, 32 devices: a whole 2x2x4 slice. The times are simulated.
32 devices in a mesh: sp: 16 (over z, y, x), tp: 2 (over core).
Axes of the slice: x: 2, y: 2, z: 4, core: 2. Of those that a mesh axis runs over, the one named last changes fastest.
Arguments:
- resid: bfloat16 [6144, 2048], P('sp'), may hold values from -6 to 6
- x_branch: bfloat16 [6144, 2048], P('sp', 'tp'), may hold values from -6 to 6
- gate_branch: bfloat16 [6144, 2048], P('sp', 'tp'), may hold values from -6 to 6
- conv_w: float32 [4, 2048], P(None, 'tp'), may hold values from -3 to 3
- gate_a_w: bfloat16 [32, 64, 64], P('tp'), may hold values from -0.75 to 0.75
- gate_x_w: bfloat16 [32, 64, 64], P('tp'), may hold values from -0.75 to 0.75
- decay_rate: float32 [2048], P('tp'), may hold values from 0 to 0.01, as said below
- decay_extra: float32 [6144, 2048], P('sp', 'tp'), may hold values from -3 to 0, as said below
- w_proj: bfloat16 [2048, 2048], P('tp'), may hold values from -0.125 to 0.125
- mix_gain: float32 [2048], replicated, may hold values from 0.1 to 1.9
- pre_gain: float32 [2048], replicated, may hold values from 0.1 to 1.9
- w_gate: bfloat16 [2048, 5632], P('sp', 'tp'), may hold values from -0.125 to 0.125
- w_up: bfloat16 [2048, 5632], P('sp', 'tp'), may hold values from -0.125 to 0.125
- w_down: bfloat16 [5632, 2048], P('tp', 'sp'), may hold values from -0.078125 to 0.078125
- out_gain: float32 [2048], replicated, may hold values from 0.1 to 1.9
Outputs:
- stream_out: bfloat16 [6144, 2048], P(('sp', 'tp'))
Inputs may be any that keep to these rules, and one draw needn't show every extreme that they name: `decay_rate`: positive rates. `decay_extra`: non-positive values.
All inputs are finite; a program needn't handle non-finite values.
Results may differ from a plain program's by a relative error of at most 0.015.
Values may be sent and summed in bfloat16 or wider, within the bound.
A program may use at most 128 MiB of HBM per device.

v0:
```python
import jax
import jax.numpy as jnp
from jax import lax
from jax.sharding import PartitionSpec as P

LRU_SCALE = 8.0
NORM_EPS = 1e-06


def from_behind(value, axis, steps):
    count = lax.axis_size(axis)
    first, last = (max(0, -steps), min(count, count - steps))
    return lax.ppermute(value, axis, [(source, source + steps) for source in range(first, last)])


def prefix(part, axis, combine, identity):
    place = lax.axis_index(axis)
    gathered = jax.tree.map(lambda a: lax.all_gather(a, axis), part)
    state = jax.tree.map(lambda a, e: jnp.zeros_like(a) + jnp.asarray(e, a.dtype), part, identity)

    def one(turn, state):
        return combine(
            state, jax.tree.map(lambda a: lax.dynamic_index_in_dim(a, turn, 0, False), gathered)
        )

    return lax.fori_loop(0, place, one, state)


def chain(earlier, later):
    return (earlier[0] * later[0], later[0] * earlier[1] + later[1])


def rms_scale(values, gains):
    return values * lax.rsqrt(jnp.mean(values * values, axis=-1, keepdims=True) + NORM_EPS) * gains


def shards(
    resid,
    x_branch,
    gate_branch,
    conv_w,
    gate_a_w,
    gate_x_w,
    decay_rate,
    decay_extra,
    w_proj,
    mix_gain,
    pre_gain,
    w_gate,
    w_up,
    w_down,
    out_gain,
):
    length = x_branch.shape[0]
    width = x_branch.shape[1]
    taps = conv_w.shape[0]
    before = from_behind(x_branch[length - (taps - 1) :], "sp", 1)
    padded = jnp.concatenate([before, x_branch], axis=0).astype(jnp.float32)
    conv = padded[0:length] * conv_w[0]
    for tap in range(1, taps):
        conv = conv + padded[tap : tap + length] * conv_w[tap]
    conv_out = conv.astype(jnp.bfloat16)
    nblocks = gate_a_w.shape[0]
    grouped = conv_out.reshape(length, nblocks, gate_a_w.shape[1])
    recur = jax.nn.sigmoid(
        jnp.einsum("rnc,ncd->rnd", grouped, gate_a_w, preferred_element_type=jnp.float32).reshape(
            length, width
        )
    )
    inject = jax.nn.sigmoid(
        jnp.einsum("rnc,ncd->rnd", grouped, gate_x_w, preferred_element_type=jnp.float32).reshape(
            length, width
        )
    )
    log_decay = -LRU_SCALE * recur * decay_rate + decay_extra
    decay = jnp.exp(log_decay)
    drive = jnp.sqrt(-jnp.expm1(2.0 * log_decay)) * inject * conv_out.astype(jnp.float32)
    prod_local, state_local = lax.associative_scan(chain, (decay, drive), axis=0)
    identity = (jnp.ones((width,), jnp.float32), jnp.zeros((width,), jnp.float32))
    carried = prefix((prod_local[-1], state_local[-1]), "sp", chain, identity)
    state = state_local + prod_local * carried[1][None, :]
    mixer = (state * jax.nn.gelu(gate_branch.astype(jnp.float32))).astype(jnp.bfloat16)
    share_rows = length // lax.axis_size("tp")
    first = lax.axis_index("tp") * share_rows
    mixed = lax.psum(
        jnp.dot(mixer, w_proj, preferred_element_type=jnp.float32).astype(jnp.bfloat16), "tp"
    ).astype(jnp.float32)
    stream = resid.astype(jnp.float32) + rms_scale(mixed, mix_gain)
    normed = rms_scale(stream, pre_gain).astype(jnp.bfloat16)
    after_mix = lax.dynamic_slice_in_dim(stream, first, share_rows, 0)
    gate_full, up_full = (
        lax.all_gather(w_gate, "sp", axis=0, tiled=True),
        lax.all_gather(w_up, "sp", axis=0, tiled=True),
    )
    down_full = lax.all_gather(w_down, "sp", axis=1, tiled=True)
    gate = jnp.dot(normed, gate_full, preferred_element_type=jnp.float32)
    upward = jnp.dot(normed, up_full, preferred_element_type=jnp.float32)
    hidden = (jax.nn.silu(gate) * upward).astype(jnp.bfloat16)
    ffn = lax.psum_scatter(
        jnp.dot(hidden, down_full, preferred_element_type=jnp.float32).astype(jnp.bfloat16),
        "tp",
        scatter_dimension=0,
        tiled=True,
    ).astype(jnp.float32)
    return (after_mix + 0.5 * rms_scale(ffn, out_gain)).astype(jnp.bfloat16)


def solution(mesh):
    return jax.shard_map(
        shards,
        mesh=mesh,
        in_specs=(
            P("sp", None),
            P("sp", "tp"),
            P("sp", "tp"),
            P(None, "tp"),
            P("tp", None, None),
            P("tp", None, None),
            P("tp"),
            P("sp", "tp"),
            P("tp", None),
            P(),
            P(),
            P("sp", "tp"),
            P("sp", "tp"),
            P("tp", "sp"),
            P(),
        ),
        out_specs=P(("sp", "tp"), None),
        check_vma=False,
    )
```

profile of v0, /device:TPU:0, one launch (start us, length us, event | category | flops | bytes accessed | tf_op | source)
XLA Modules:
  0.0 737.7 jit_solution(13793167642620603508)
XLA Ops:
  8.1 4.9 collective-permute-start
  17.8 1.8 add_divide_fusion.1
  19.6 1.7 copy.106
  21.3 1.8 add_divide_fusion
  23.0 1.6 copy.108
  24.6 5.3 convert_multiply_fusion.7
  30.0 4.5 slice.281
  34.4 2.1 slice.282
  36.6 2.1 slice.280
  38.7 2.2 slice.284
  40.9 3.4 multiply_add_fusion.2
  44.2 2.7 slice.287
  46.9 2.7 slice.288
  49.6 2.7 slice.286
  52.4 2.7 slice.290
  55.1 2.4 multiply_add_fusion.3
  57.4 1.7 slice.293
  59.1 1.7 slice.294
  60.8 1.7 slice.292
  62.5 1.7 slice.296
  64.1 2.0 multiply_add_fusion.4
  67.4 1.6 slice.298
  69.0 1.6 slice.302
  70.6 1.7 multiply_add_fusion.5
  76.6 1.6 multiply_add_fusion.6
  102.2 1.7 slice.291
  103.9 1.7 slice.334
  108.2 2.7 slice.285
  111.0 2.8 slice.336
  116.5 2.3 slice.279
  118.8 2.2 slice.338
  128.0 3.1 pad.113
  135.6 3.2 pad.112
  139.6 42.0 %all-gather.1 = f32[16,1,1024]{2,1,0:T(1,128)S(1)} all-gather(f32[1,1,1024]{2,1,0:T(1,128)S(1)} %add_bitcast_fusion), channel_id=1, replica_groups=mesh['sp'=16,'tp'=2] {'sp'}, dimensions={0}, use_global_device_ids=true | all-gather | bytes 69632 | tf_op jit(solution)/shard_map/all_gather | solution.py:18
  181.7 3.1 pad.129
  184.9 3.2 pad.128
  188.9 35.8 %all-gather = f32[16,1,1024]{2,1,0:T(1,128)S(1)} all-gather(f32[1,1,1024]{2,1,0:T(1,128)S(1)} %add_bitcast_fusion.1), channel_id=1, replica_groups=mesh['sp'=16,'tp'=2] {'sp'}, dimensions={0}, use_global_device_ids=true | all-gather | bytes 69632 | tf_op jit(solution)/shard_map/all_gather | solution.py:18
  224.7 7.0 convolution_convert_fusion.1
  233.6 17.4 %all-reduce.34.cloned.1.call-done = bf16[384,2048]{1,0:T(8,128)(2,1)} async-done(((bf16[384,2048]{1,0:T(8,128)(2,1)}), bf16[384,2048]{1,0:T(8,128)(2,1)}) %all-reduce.34.cloned.1.call-update) | async-done | bytes 1572880 | tf_op jit(solution)/shard_map/psum | solution.py:85
  250.9 1.9 fusion.1
  252.9 2.3 multiply_reduce_fusion
  255.2 119.6 %all-gather.6.cloned.1.call-done = bf16[2048,2816]{1,0:T(8,128)(2,1)} async-done(((bf16[128,2816]{1,0:T(8,128)(2,1)}), bf16[2048,2816]{1,0:T(8,128)(2,1)}) %all-gather.6.cloned.1.call-update) | async-done | bytes 11534352 | tf_op jit(solution)/shard_map/all_gather | solution.py:92
  374.9 9.6 %fusion.43 = f32[384,2816]{1,0:T(8,128)} fusion(bf16[2048,2816]{1,0:T(8,128)(2,1)} %all-gather.6.cloned.1.call-done, f32[384,2048]{1,0:T(8,128)S(1)} %get-tuple-element.61, f32[2048]{0:T(1024)S(1)} %copy-done.38, f32[384]{0:T(512)S(1)} %add_rsqrt_fusion), kind=kOutput, calls=%fused_computation.118 | convolution fusion | flops 4431544320 | bytes 19015168 | tf_op jit(solution)/shard_map/dot_general | solution.py:96
  384.4 173.1 %all-gather.10.cloned.1.call-done = bf16[2816,2048]{1,0:T(8,128)(2,1)} async-done(((bf16[2816,128]{1,0:T(8,128)(2,1)}), bf16[2816,2048]{1,0:T(8,128)(2,1)}) %all-gather.10.cloned.1.call-update) | async-done | bytes 11534352 | tf_op jit(solution)/shard_map/all_gather | solution.py:95
  557.5 142.0 %all-gather.8.cloned.1.call-done = bf16[2048,2816]{1,0:T(8,128)(2,1)} async-done(((bf16[128,2816]{1,0:T(8,128)(2,1)}), bf16[2048,2816]{1,0:T(8,128)(2,1)}) %all-gather.8.cloned.1.call-update) | async-done | bytes 11534352 | tf_op jit(solution)/shard_map/all_gather | solution.py:93
  699.5 19.3 %convolution_convert_fusion = bf16[384,2048]{1,0:T(8,128)(2,1)} fusion(bf16[2816,2048]{1,0:T(8,128)(2,1)} %all-gather.10.cloned.1.call-done, bf16[2048,2816]{1,0:T(8,128)(2,1)} %all-gather.8.cloned.1.call-done, f32[384,2816]{1,0:T(8,128)} %fusion.43, f32[384,2048]{1,0:T(8,128)S(1)} %get-tuple-element.61, f32[2048]{0:T(1024)S(1)} %copy-done.38, ...), kind=kOutput, calls=%fused_computation.12 | convolution fusion | flops 8868003840 | bytes 32122368 | tf_op jit(solution)/shard_map/dot_general | solution.py:100
  718.9 7.4 reduce-scatter.2.cloned.1.call-done
  727.7 2.4 fusion.8
  (205 shorter events, 56.4 us)
Async XLA Ops:
  7.4 10.4 %copy-start = (bf16[16,64,64]{2,1,0:T(8,128)(2,1)S(1)}, bf16[16,64,64]{2,1,0:T(8,128)(2,1)}, u32[]{:S(2)}) copy-start(bf16[16,64,64]{2,1,0:T(8,128)(2,1)} %param.21) | copy-start | bytes 393220
  7.4 243.6 %all-reduce.34.cloned.1.call-start = ((), (), s32[]{:S(2)}) async-start(), calls=%async_computation.1 | async-start | bytes 3145728 | tf_op jit(solution)/shard_map/psum | solution.py:85
  8.1 6.5 collective-permute-start
  19.6 1.7 copy-start.37
  29.9 4.5 copy-start.2
  116.5 5.7 copy-start.15
  116.5 5.7 copy-start.16
  116.5 5.7 copy-start.17
  116.5 6.0 copy-start.18
  116.5 6.0 copy-start.19
  116.5 6.0 copy-start.26
  116.5 6.0 copy-start.27
  118.8 3.8 copy-start.14
  118.8 3.9 copy-start.33
  118.8 3.9 copy-start.32
  121.6 2.1 copy-start.31
  122.2 1.6 copy-start.30
  122.6 1.3 copy-start.13
  122.8 1.2 copy-start.29
  123.7 0.7 copy-start.28
  124.0 0.9 copy-start.11
  124.0 1.0 copy-start.12
  124.5 0.7 copy-start.25
  125.0 0.7 copy-start.24
  125.7 1.0 copy-start.9
  125.7 1.2 copy-start.10
  126.9 0.7 copy-start.23
  128.0 3.1 copy-start.22
  132.5 1.4 copy-start.4
  132.5 1.6 copy-start.5
  134.1 1.4 copy-start.21
  135.6 3.2 copy-start.8
  135.6 46.1 %copy-start.7 = (f32[192,1024]{1,0:T(8,128)S(1)}, f32[192,1024]{1,0:T(8,128)}, u32[]{:S(2)}) copy-start(f32[192,1024]{1,0:T(8,128)} %add.291) | copy-start | bytes 2359300
  138.8 46.0 %copy-start.6 = (f32[191,1024]{1,0:T(8,128)S(1)}, f32[191,1024]{1,0:T(8,128)}, u32[]{:S(2)}) copy-start(f32[191,1024]{1,0:T(8,128)} %get-tuple-element.71) | copy-start | bytes 2347012
  138.8 46.0 %copy-start.20 = (f32[1,1024]{1,0:T(1,128)S(1)}, f32[1,1024]{1,0:T(1,128)}, u32[]{:S(2)}) copy-start(f32[1,1024]{1,0:T(1,128)} %slice.386) | copy-start | bytes 12292
  184.9 39.8 %copy-start.36 = (bf16[384,1024]{1,0:T(8,128)(2,1)S(1)}, bf16[384,1024]{1,0:T(8,128)(2,1)}, u32[]{:S(2)}) copy-start(bf16[384,1024]{1,0:T(8,128)(2,1)} %param.19) | copy-start | bytes 2359300
  231.8 143.1 %all-gather.6.cloned.1.call-start = ((), (), s32[]{:S(2)}) async-start(), calls=%async_computation.2 | async-start | bytes 12255232 | tf_op jit(solution)/shard_map/all_gather | solution.py:92
  232.3 20.5 %copy-start.34 = (f32[2048]{0:T(1024)S(1)}, f32[2048]{0:T(1024)}, u32[]{:S(2)}) copy-start(f32[2048]{0:T(1024)} %param.26) | copy-start | bytes 24580
  232.3 325.2 %all-gather.10.cloned.1.call-start = ((), (), s32[]{:S(2)}) async-start(), calls=%async_computation.4 | async-start | bytes 12255232 | tf_op jit(solution)/shard_map/all_gather | solution.py:95
  232.9 466.6 %all-gather.8.cloned.1.call-start = ((), (), s32[]{:S(2)}) async-start(), calls=%async_computation.3 | async-start | bytes 12255232 | tf_op jit(solution)/shard_map/all_gather | solution.py:93
  233.5 492.8 %reduce-scatter.2.cloned.1.call-start = ((), (), s32[]{:S(2)}) async-start(), calls=%async_computation.5 | async-start | bytes 2359296 | tf_op jit(solution)/shard_map/reduce_scatter | solution.py:99
  250.9 1.9 copy-start.3
  252.9 122.0 %copy-start.38 = (f32[2048]{0:T(1024)S(1)}, f32[2048]{0:T(1024)}, u32[]{:S(2)}) copy-start(f32[2048]{0:T(1024)} %param.27) | copy-start | bytes 24580
  718.9 8.8 %copy-start.35 = (f32[2048]{0:T(1024)S(1)}, f32[2048]{0:T(1024)}, u32[]{:S(2)}) copy-start(f32[2048]{0:T(1024)} %param.31) | copy-start | bytes 24580
  727.7 2.4 copy-start.1
Sparse Core Ops, SparseCore 0:
  231.9 19.0 all-reduce.33
  719.0 7.2 reduce-scatter.1
Sparse Core Ops, SparseCore 1:
  235.0 139.8 all-gather.5
  377.4 180.0 all-gather.9
  560.1 139.3 all-gather.7
where the time goes:
time: 740 us; the launch traced here: 738 us
  waiting for transfers between devices  461 us (62%)
  local copies, waits for them, and re-layouts  103 us (14%)
  blocking collectives  77.8 us (11%)
  matrix products  39.4 us (5%)
  other arithmetic  35.2 us (5%)
  between operations  15.9 us (2%)
    all_gather x1, waiting for transfers between devices, shards(): down_full = lax.all_gather(w_down, 'sp', axis=1, tiled=True)  173 us
    all_gather x1, waiting for transfers between devices, shards(): lax.all_gather(w_up, 'sp', axis=0, tiled=True)  142 us
    all_gather x1, waiting for transfers between devices, shards(): lax.all_gather(w_gate, 'sp', axis=0, tiled=True)  120 us
    slice x56, local copies, waits for them, and re-layouts, shards(): lax.associative_scan(chain, (decay, drive), axis=0)  79.8 us
    all_gather x2, blocking collectives, prefix(): gathered = jax.tree.map(lambda a: lax.all_gather(a, axis), part)  77.8 us
    dot_general x1, matrix products, shards(): jnp.dot(hidden, down_full, preferred_element_type=jnp.float32)  19.3 us
    psum x1, waiting for transfers between devices, shards(): lax.psum(jnp.dot(mixer, w_proj, preferred_element_type=jnp.float32).astyp...  17.4 us
    add x15, other arithmetic, chain(): return (earlier[0] * later[0], later[0] * earlier[1] + later[1])  15 us
  transfers between devices with their start and end apart: 6, of which 5 were waited for; matrix products, arithmetic and copies ran while one was open for 2% of the time, Pallas kernels for 0%

commit v1 on v0

--- a/solution.py
+++ b/solution.py
@@ -92,7 +92,14 @@
         lax.all_gather(w_gate, "sp", axis=0, tiled=True),
         lax.all_gather(w_up, "sp", axis=0, tiled=True),
     )
-    down_full = lax.all_gather(w_down, "sp", axis=1, tiled=True)
+    world_n = jax.lax.axis_size("sp")
+    arr_out = [None] * world_n
+    arr_out[world_n - 1] = w_down
+    parts_seen = tuple(((it, (it + 1) % world_n) for it in range(world_n)))
+    for q in range(world_n - 2, -1, -1):
+        arr_out[q] = jax.lax.ppermute(arr_out[q + 1], "sp", perm=parts_seen)
+    odd = jnp.concatenate(arr_out, axis=1)
+    down_full = jnp.roll(odd, shift=(jax.lax.axis_index("sp") + 1) * w_down.shape[1], axis=1)
     gate = jnp.dot(normed, gate_full, preferred_element_type=jnp.float32)
     upward = jnp.dot(normed, up_full, preferred_element_type=jnp.float32)
     hidden = (jax.nn.silu(gate) * upward).astype(jnp.bfloat16)

time: 740 us -> 783 us (1.058)
  local copies, waits for them, and re-layouts: 103 us -> 140 us
  other arithmetic: 35.2 us -> 45.1 us
    ppermute x0 -> x15, waiting for transfers between devices: none -> 449 us  [shards(): arr_out[q] = jax.lax.ppermute(arr_out[q + 1], 'sp', perm=parts_seen)]
    all_gather x1 -> x0, waiting for transfers between devices: 173 us -> none  [shards(): down_full = lax.all_gather(w_down, 'sp', axis=1, tiled=True)]
    all_gather x1, waiting for transfers between devices: 142 us -> 0.01 us  [shards(): lax.all_gather(w_up, 'sp', axis=0, tiled=True)]
    all_gather x1, waiting for transfers between devices: 120 us -> 0.01 us  [shards(): lax.all_gather(w_gate, 'sp', axis=0, tiled=True)]
    unnamed x80 -> x147, local copies, waits for them, and re-layouts: 2.7 us -> 41.7 us
    psum x1, waiting for transfers between devices: 17.4 us -> 0.01 us  [shards(): lax.psum(jnp.dot(mixer, w_proj, preferred_element_type=jnp.float32).astyp...]
  transfers between devices with their start and end apart: 6 -> 20, of which waited for: 5 -> 16; matrix products, arithmetic and copies ran while one was open for 2% -> 6% of each run, Pallas kernels for 0% -> 0%
where the time goes in v1:
time: 783 us; the launch traced here: 780 us
  waiting for transfers between devices  455 us (58%)
  local copies, waits for them, and re-layouts  140 us (18%)
  blocking collectives  77.8 us (10%)
  other arithmetic  45.1 us (6%)
  matrix products  39.9 us (5%)
  between operations  15.6 us (2%)
    ppermute x15, waiting for transfers between devices, shards(): arr_out[q] = jax.lax.ppermute(arr_out[q + 1], 'sp', perm=parts_seen)  449 us
    slice x56, local copies, waits for them, and re-layouts, shards(): lax.associative_scan(chain, (decay, drive), axis=0)  78 us
    all_gather x2, blocking collectives, prefix(): gathered = jax.tree.map(lambda a: lax.all_gather(a, axis), part)  77.8 us
    unnamed x147, local copies, waits for them, and re-layouts  41.7 us
    dot_general x1, matrix products, shards(): jnp.dot(hidden, down_full, preferred_element_type=jnp.float32)  19.3 us
    add x15, other arithmetic, chain(): return (earlier[0] * later[0], later[0] * earlier[1] + later[1])  18 us
  transfers between devices with their start and end apart: 20, of which 16 were waited for; matrix products, arithmetic and copies ran while one was open for 6% of the time, Pallas kernels for 0%

profile of v1, /device:TPU:0, one launch (start us, length us, event | category | flops | bytes accessed | tf_op | source)
XLA Modules:
  0.0 780.1 jit_solution(17684429321763095183)
XLA Ops:
  8.1 4.9 collective-permute-start
  17.8 1.8 add_divide_fusion
  24.6 5.3 convert_multiply_fusion.7
  29.9 2.2 slice.338
  32.2 2.1 slice.282
  34.3 2.2 slice.279
  36.5 2.1 slice.280
  38.7 2.2 slice.281
  40.8 2.1 slice.284
  43.0 3.4 multiply_add_fusion.2
  46.4 2.7 slice.288
  49.1 2.7 slice.287
  51.8 2.7 slice.286
  54.5 2.7 slice.290
  57.2 2.4 multiply_add_fusion.3
  69.7 1.9 multiply_add_fusion.4
  109.6 2.7 slice.336
  112.4 2.7 slice.285
  138.9 3.1 pad.128
  142.0 3.2 pad.129
  145.4 3.1 pad.112
  149.6 41.8 %all-gather = f32[16,1,1024]{2,1,0:T(1,128)S(1)} all-gather(f32[1,1,1024]{2,1,0:T(1,128)S(1)} %add_bitcast_fusion.1), channel_id=1, replica_groups=mesh['sp'=16,'tp'=2] {'sp'}, dimensions={0}, use_global_device_ids=true | all-gather | bytes 69632 | tf_op jit(solution)/shard_map/all_gather | solution.py:18
  192.2 35.9 %all-gather.1 = f32[16,1,1024]{2,1,0:T(1,128)S(1)} all-gather(f32[1,1,1024]{2,1,0:T(1,128)S(1)} %add_bitcast_fusion), channel_id=1, replica_groups=mesh['sp'=16,'tp'=2] {'sp'}, dimensions={0}, use_global_device_ids=true | all-gather | bytes 69632 | tf_op jit(solution)/shard_map/all_gather | solution.py:18
  228.4 7.5 convolution_convert_fusion
  236.6 2.1 collective-permute-start.1
  238.7 24.5 %collective-permute-done.1 = bf16[2816,128]{1,0:T(8,128)(2,1)S(1)} collective-permute-done((bf16[2816,128]{1,0:T(8,128)(2,1)S(1)}, bf16[2816,128]{1,0:T(8,128)(2,1)S(1)}, u32[]{:S(2)}, u32[]{:S(2)}) %collective-permute-start.1) | collective-permute-done | bytes 720928 | tf_op jit(solution)/shard_map/ppermute | solution.py:100
  264.1 24.5 %collective-permute-done.2 = bf16[2816,128]{1,0:T(8,128)(2,1)S(1)} collective-permute-done((bf16[2816,128]{1,0:T(8,128)(2,1)S(1)}, bf16[2816,128]{1,0:T(8,128)(2,1)S(1)}, u32[]{:S(2)}, u32[]{:S(2)}) %collective-permute-start.2) | collective-permute-done | bytes 720928 | tf_op jit(solution)/shard_map/ppermute | solution.py:100
  288.7 36.2 %collective-permute-done.3 = bf16[2816,128]{1,0:T(8,128)(2,1)S(1)} collective-permute-done((bf16[2816,128]{1,0:T(8,128)(2,1)S(1)}, bf16[2816,128]{1,0:T(8,128)(2,1)S(1)}, u32[]{:S(2)}, u32[]{:S(2)}) %collective-permute-start.3) | collective-permute-done | bytes 720928 | tf_op jit(solution)/shard_map/ppermute | solution.py:100
  324.9 26.7 %collective-permute-done.4 = bf16[2816,128]{1,0:T(8,128)(2,1)S(1)} collective-permute-done((bf16[2816,128]{1,0:T(8,128)(2,1)S(1)}, bf16[2816,128]{1,0:T(8,128)(2,1)S(1)}, u32[]{:S(2)}, u32[]{:S(2)}) %collective-permute-start.4) | collective-permute-done | bytes 720928 | tf_op jit(solution)/shard_map/ppermute | solution.py:100
  352.5 37.5 %collective-permute-done.5 = bf16[2816,128]{1,0:T(8,128)(2,1)S(1)} collective-permute-done((bf16[2816,128]{1,0:T(8,128)(2,1)S(1)}, bf16[2816,128]{1,0:T(8,128)(2,1)S(1)}, u32[]{:S(2)}, u32[]{:S(2)}) %collective-permute-start.5) | collective-permute-done | bytes 720928 | tf_op jit(solution)/shard_map/ppermute | solution.py:100
  390.8 34.3 %collective-permute-done.6 = bf16[2816,128]{1,0:T(8,128)(2,1)S(1)} collective-permute-done((bf16[2816,128]{1,0:T(8,128)(2,1)S(1)}, bf16[2816,128]{1,0:T(8,128)(2,1)S(1)}, u32[]{:S(2)}, u32[]{:S(2)}) %collective-permute-start.6) | collective-permute-done | bytes 720928 | tf_op jit(solution)/shard_map/ppermute | solution.py:100
  426.0 36.8 %collective-permute-done.7 = bf16[2816,128]{1,0:T(8,128)(2,1)S(1)} collective-permute-done((bf16[2816,128]{1,0:T(8,128)(2,1)S(1)}, bf16[2816,128]{1,0:T(8,128)(2,1)S(1)}, u32[]{:S(2)}, u32[]{:S(2)}) %collective-permute-start.7) | collective-permute-done | bytes 720928 | tf_op jit(solution)/shard_map/ppermute | solution.py:100
  463.6 29.2 %collective-permute-done.8 = bf16[2816,128]{1,0:T(8,128)(2,1)S(1)} collective-permute-done((bf16[2816,128]{1,0:T(8,128)(2,1)S(1)}, bf16[2816,128]{1,0:T(8,128)(2,1)S(1)}, u32[]{:S(2)}, u32[]{:S(2)}) %collective-permute-start.8) | collective-permute-done | bytes 720928 | tf_op jit(solution)/shard_map/ppermute | solution.py:100
  493.7 25.1 %collective-permute-done.9 = bf16[2816,128]{1,0:T(8,128)(2,1)S(1)} collective-permute-done((bf16[2816,128]{1,0:T(8,128)(2,1)S(1)}, bf16[2816,128]{1,0:T(8,128)(2,1)S(1)}, u32[]{:S(2)}, u32[]{:S(2)}) %collective-permute-start.9) | collective-permute-done | bytes 720928 | tf_op jit(solution)/shard_map/ppermute | solution.py:100
  519.7 33.7 %collective-permute-done.10 = bf16[2816,128]{1,0:T(8,128)(2,1)S(1)} collective-permute-done((bf16[2816,128]{1,0:T(8,128)(2,1)S(1)}, bf16[2816,128]{1,0:T(8,128)(2,1)S(1)}, u32[]{:S(2)}, u32[]{:S(2)}) %collective-permute-start.10) | collective-permute-done | bytes 720928 | tf_op jit(solution)/shard_map/ppermute | solution.py:100
  554.2 23.1 %collective-permute-done.11 = bf16[2816,128]{1,0:T(8,128)(2,1)S(1)} collective-permute-done((bf16[2816,128]{1,0:T(8,128)(2,1)S(1)}, bf16[2816,128]{1,0:T(8,128)(2,1)S(1)}, u32[]{:S(2)}, u32[]{:S(2)}) %collective-permute-start.11) | collective-permute-done | bytes 720928 | tf_op jit(solution)/shard_map/ppermute | solution.py:100
  578.2 37.2 %collective-permute-done.12 = bf16[2816,128]{1,0:T(8,128)(2,1)S(1)} collective-permute-done((bf16[2816,128]{1,0:T(8,128)(2,1)S(1)}, bf16[2816,128]{1,0:T(8,128)(2,1)S(1)}, u32[]{:S(2)}, u32[]{:S(2)}) %collective-permute-start.12) | collective-permute-done | bytes 720928 | tf_op jit(solution)/shard_map/ppermute | solution.py:100
  616.3 33.1 %collective-permute-done.13 = bf16[2816,128]{1,0:T(8,128)(2,1)S(1)} collective-permute-done((bf16[2816,128]{1,0:T(8,128)(2,1)S(1)}, bf16[2816,128]{1,0:T(8,128)(2,1)S(1)}, u32[]{:S(2)}, u32[]{:S(2)}) %collective-permute-start.13) | collective-permute-done | bytes 720928 | tf_op jit(solution)/shard_map/ppermute | solution.py:100
  649.4 2.1 fusion.3
  651.5 34.9 %collective-permute-done.14 = bf16[2816,128]{1,0:T(8,128)(2,1)} collective-permute-done((bf16[2816,128]{1,0:T(8,128)(2,1)S(1)}, bf16[2816,128]{1,0:T(8,128)(2,1)}, u32[]{:S(2)}, u32[]{:S(2)}) %collective-permute-start.14) | collective-permute-done | bytes 720928 | tf_op jit(solution)/shard_map/ppermute | solution.py:100
  686.5 2.8 multiply_reduce_fusion
  689.3 12.2 %collective-permute-done.15 = bf16[2816,128]{1,0:T(8,128)(2,1)S(1)} collective-permute-done((bf16[2816,128]{1,0:T(8,128)(2,1)}, bf16[2816,128]{1,0:T(8,128)(2,1)S(1)}, u32[]{:S(2)}, u32[]{:S(2)}) %collective-permute-start.15) | collective-permute-done | bytes 720928 | tf_op jit(solution)/shard_map/ppermute | solution.py:100
  702.5 2.1 constant_dynamic-update-slice_fusion.30
  719.2 2.1 constant_dynamic-update-slice_fusion.14
  734.9 9.5 %fusion.49 = f32[384,2816]{1,0:T(8,128)} fusion(bf16[2048,2816]{1,0:T(8,128)(2,1)} %all-gather.5.cloned.1.call-done, f32[384,2048]{1,0:T(8,128)S(1)} %get-tuple-element.61, f32[2048]{0:T(1024)S(1)} %copy-done.56, f32[384]{0:T(512)S(1)} %add_rsqrt_fusion), kind=kOutput, calls=%fused_computation.153 | convolution fusion | flops 4431544320 | bytes 19015168 | tf_op jit(solution)/shard_map/dot_general | solution.py:103
  744.4 19.3 %fusion.6 = bf16[384,2048]{1,0:T(8,128)(2,1)} fusion(bf16[2816,4096]{1,0:T(8,128)(2,1)} %constant_dynamic-update-slice_fusion, s32[]{:T(128)S(6)} %select_n.24, bf16[2048,2816]{1,0:T(8,128)(2,1)} %all-gather.7.cloned.1.call-done, f32[384,2816]{1,0:T(8,128)} %fusion.49, f32[384,2048]{1,0:T(8,128)S(1)} %get-tuple-element.61, f32[2048]{0:T(1024)S(1)} %copy-done.56, ...), kind=kOutput, calls=%fused_computation.14 | convolution fusion | flops 8868003840 | bytes 32122372 | tf_op jit(solution)/shard_map/dot_general | solution.py:107
  763.8 5.1 reduce-scatter.2.cloned.1.call-done
  770.3 2.4 fusion.13
  (300 shorter events, 124.1 us)
Async XLA Ops:
  7.4 10.4 %copy-start = (bf16[16,64,64]{2,1,0:T(8,128)(2,1)S(1)}, bf16[16,64,64]{2,1,0:T(8,128)(2,1)}, u32[]{:S(2)}) copy-start(bf16[16,64,64]{2,1,0:T(8,128)(2,1)} %param.22) | copy-start | bytes 393220
  7.4 642.1 %all-reduce.34.cloned.1.call-start = ((), (), s32[]{:S(2)}) async-start(), calls=%async_computation.1 | async-start | bytes 3145728 | tf_op jit(solution)/shard_map/psum | solution.py:85
  8.1 6.5 collective-permute-start
  29.9 4.4 copy-start.2
  106.4 20.6 %copy-start.43 = (f32[23,1024]{1,0:T(8,128)S(1)}, f32[23,1024]{1,0:T(8,128)}, u32[]{:S(2)}) copy-start(f32[23,1024]{1,0:T(8,128)} %slice.332) | copy-start | bytes 282628
  119.8 7.2 copy-start.51
  119.8 7.2 copy-start.44
  124.3 4.9 copy-start.40
  124.4 4.9 copy-start.41
  138.8 6.4 copy-start.5
  138.8 6.4 copy-start.45
  142.0 6.5 copy-start.6
  145.4 83.0 %copy-start.54 = (bf16[384,1024]{1,0:T(8,128)(2,1)S(1)}, bf16[384,1024]{1,0:T(8,128)(2,1)}, u32[]{:S(2)}) copy-start(bf16[384,1024]{1,0:T(8,128)(2,1)} %param.19) | copy-start | bytes 2359300
  148.7 79.6 %copy-start.36 = (f32[384,1024]{1,0:T(8,128)}, f32[384,1024]{1,0:T(8,128)S(1)}, u32[]{:S(2)}) copy-start(f32[384,1024]{1,0:T(8,128)S(1)} %pad.113) | copy-start | bytes 4718596
  228.4 8.2 %copy-start.8 = (bf16[2816,128]{1,0:T(8,128)(2,1)S(1)}, bf16[2816,128]{1,0:T(8,128)(2,1)}, u32[]{:S(2)}) copy-start(bf16[2816,128]{1,0:T(8,128)(2,1)} %param.30) | copy-start | bytes 2162692
  235.9 450.5 %copy-start.52 = (f32[2048]{0:T(1024)S(1)}, f32[2048]{0:T(1024)}, u32[]{:S(2)}) copy-start(f32[2048]{0:T(1024)} %param.26) | copy-start | bytes 24580
  235.9 499.0 %all-gather.5.cloned.1.call-start = ((), (), s32[]{:S(2)}) async-start(), calls=%async_computation.2 | async-start | bytes 12255232 | tf_op jit(solution)/shard_map/all_gather | solution.py:92
  236.5 507.9 %all-gather.7.cloned.1.call-start = ((), (), s32[]{:S(2)}) async-start(), calls=%async_computation.3 | async-start | bytes 12255232 | tf_op jit(solution)/shard_map/all_gather | solution.py:93
  236.6 26.7 %collective-permute-start.1 = (bf16[2816,128]{1,0:T(8,128)(2,1)S(1)}, bf16[2816,128]{1,0:T(8,128)(2,1)S(1)}, u32[]{:S(2)}, u32[]{:S(2)}) collective-permute-start(bf16[2816,128]{1,0:T(8,128)(2,1)S(1)} %copy-done.8), channel_id=1, source_target_pairs={{0,2},{2,4},{4,6},{6,8},{8,10},{10,12},{12,14},{14,16},{16,18},{18... | collective-permute-start | bytes 2162696 | tf_op jit(solution)/shard_map/ppermute | solution.py:100
  264.1 24.5 %collective-permute-start.2 = (bf16[2816,128]{1,0:T(8,128)(2,1)S(1)}, bf16[2816,128]{1,0:T(8,128)(2,1)S(1)}, u32[]{:S(2)}, u32[]{:S(2)}) collective-permute-start(bf16[2816,128]{1,0:T(8,128)(2,1)S(1)} %collective-permute-done.1), channel_id=1, source_target_pairs={{0,2},{2,4},{4,6},{6,8},{8,10},{10,12},{12,14},{14,16},{16,18},{18... | collective-permute-start | bytes 2162696 | tf_op jit(solution)/shard_map/ppermute | solution.py:100
  288.6 397.8 %copy-start.12 = (bf16[2816,128]{1,0:T(8,128)(2,1)}, bf16[2816,128]{1,0:T(8,128)(2,1)S(1)}, u32[]{:S(2)}) copy-start(bf16[2816,128]{1,0:T(8,128)(2,1)S(1)} %collective-permute-done.2) | copy-start | bytes 2162692
  288.6 36.2 %collective-permute-start.3 = (bf16[2816,128]{1,0:T(8,128)(2,1)S(1)}, bf16[2816,128]{1,0:T(8,128)(2,1)S(1)}, u32[]{:S(2)}, u32[]{:S(2)}) collective-permute-start(bf16[2816,128]{1,0:T(8,128)(2,1)S(1)} %collective-permute-done.2), channel_id=1, source_target_pairs={{0,2},{2,4},{4,6},{6,8},{8,10},{10,12},{12,14},{14,16},{16,18},{18... | collective-permute-start | bytes 2162696 | tf_op jit(solution)/shard_map/ppermute | solution.py:100
  288.7 480.2 %reduce-scatter.2.cloned.1.call-start = ((), (), s32[]{:S(2)}) async-start(), calls=%async_computation.4 | async-start | bytes 2359296 | tf_op jit(solution)/shard_map/reduce_scatter | solution.py:106
  324.9 361.6 %copy-start.14 = (bf16[2816,128]{1,0:T(8,128)(2,1)}, bf16[2816,128]{1,0:T(8,128)(2,1)S(1)}, u32[]{:S(2)}) copy-start(bf16[2816,128]{1,0:T(8,128)(2,1)S(1)} %collective-permute-done.3) | copy-start | bytes 2162692
  324.9 26.7 %collective-permute-start.4 = (bf16[2816,128]{1,0:T(8,128)(2,1)S(1)}, bf16[2816,128]{1,0:T(8,128)(2,1)S(1)}, u32[]{:S(2)}, u32[]{:S(2)}) collective-permute-start(bf16[2816,128]{1,0:T(8,128)(2,1)S(1)} %collective-permute-done.3), channel_id=1, source_target_pairs={{0,2},{2,4},{4,6},{6,8},{8,10},{10,12},{12,14},{14,16},{16,18},{18... | collective-permute-start | bytes 2162696 | tf_op jit(solution)/shard_map/ppermute | solution.py:100
  352.5 37.5 %collective-permute-start.5 = (bf16[2816,128]{1,0:T(8,128)(2,1)S(1)}, bf16[2816,128]{1,0:T(8,128)(2,1)S(1)}, u32[]{:S(2)}, u32[]{:S(2)}) collective-permute-start(bf16[2816,128]{1,0:T(8,128)(2,1)S(1)} %collective-permute-done.4), channel_id=1, source_target_pairs={{0,2},{2,4},{4,6},{6,8},{8,10},{10,12},{12,14},{14,16},{16,18},{18... | collective-permute-start | bytes 2162696 | tf_op jit(solution)/shard_map/ppermute | solution.py:100
  390.8 34.3 %collective-permute-start.6 = (bf16[2816,128]{1,0:T(8,128)(2,1)S(1)}, bf16[2816,128]{1,0:T(8,128)(2,1)S(1)}, u32[]{:S(2)}, u32[]{:S(2)}) collective-permute-start(bf16[2816,128]{1,0:T(8,128)(2,1)S(1)} %collective-permute-done.5), channel_id=1, source_target_pairs={{0,2},{2,4},{4,6},{6,8},{8,10},{10,12},{12,14},{14,16},{16,18},{18... | collective-permute-start | bytes 2162696 | tf_op jit(solution)/shard_map/ppermute | solution.py:100
  426.0 36.8 %collective-permute-start.7 = (bf16[2816,128]{1,0:T(8,128)(2,1)S(1)}, bf16[2816,128]{1,0:T(8,128)(2,1)S(1)}, u32[]{:S(2)}, u32[]{:S(2)}) collective-permute-start(bf16[2816,128]{1,0:T(8,128)(2,1)S(1)} %collective-permute-done.6), channel_id=1, source_target_pairs={{0,2},{2,4},{4,6},{6,8},{8,10},{10,12},{12,14},{14,16},{16,18},{18... | collective-permute-start | bytes 2162696 | tf_op jit(solution)/shard_map/ppermute | solution.py:100
  463.6 29.2 %collective-permute-start.8 = (bf16[2816,128]{1,0:T(8,128)(2,1)S(1)}, bf16[2816,128]{1,0:T(8,128)(2,1)S(1)}, u32[]{:S(2)}, u32[]{:S(2)}) collective-permute-start(bf16[2816,128]{1,0:T(8,128)(2,1)S(1)} %collective-permute-done.7), channel_id=1, source_target_pairs={{0,2},{2,4},{4,6},{6,8},{8,10},{10,12},{12,14},{14,16},{16,18},{18... | collective-permute-start | bytes 2162696 | tf_op jit(solution)/shard_map/ppermute | solution.py:100
  493.7 25.1 %collective-permute-start.9 = (bf16[2816,128]{1,0:T(8,128)(2,1)S(1)}, bf16[2816,128]{1,0:T(8,128)(2,1)S(1)}, u32[]{:S(2)}, u32[]{:S(2)}) collective-permute-start(bf16[2816,128]{1,0:T(8,128)(2,1)S(1)} %collective-permute-done.8), channel_id=1, source_target_pairs={{0,2},{2,4},{4,6},{6,8},{8,10},{10,12},{12,14},{14,16},{16,18},{18... | collective-permute-start | bytes 2162696 | tf_op jit(solution)/shard_map/ppermute | solution.py:100
  519.6 33.7 %collective-permute-start.10 = (bf16[2816,128]{1,0:T(8,128)(2,1)S(1)}, bf16[2816,128]{1,0:T(8,128)(2,1)S(1)}, u32[]{:S(2)}, u32[]{:S(2)}) collective-permute-start(bf16[2816,128]{1,0:T(8,128)(2,1)S(1)} %collective-permute-done.9), channel_id=1, source_target_pairs={{0,2},{2,4},{4,6},{6,8},{8,10},{10,12},{12,14},{14,16},{16,18},{18... | collective-permute-start | bytes 2162696 | tf_op jit(solution)/shard_map/ppermute | solution.py:100
  554.2 23.1 %collective-permute-start.11 = (bf16[2816,128]{1,0:T(8,128)(2,1)S(1)}, bf16[2816,128]{1,0:T(8,128)(2,1)S(1)}, u32[]{:S(2)}, u32[]{:S(2)}) collective-permute-start(bf16[2816,128]{1,0:T(8,128)(2,1)S(1)} %collective-permute-done.10), channel_id=1, source_target_pairs={{0,2},{2,4},{4,6},{6,8},{8,10},{10,12},{12,14},{14,16},{16,18},{18... | collective-permute-start | bytes 2162696 | tf_op jit(solution)/shard_map/ppermute | solution.py:100
  578.2 37.2 %collective-permute-start.12 = (bf16[2816,128]{1,0:T(8,128)(2,1)S(1)}, bf16[2816,128]{1,0:T(8,128)(2,1)S(1)}, u32[]{:S(2)}, u32[]{:S(2)}) collective-permute-start(bf16[2816,128]{1,0:T(8,128)(2,1)S(1)} %collective-permute-done.11), channel_id=1, source_target_pairs={{0,2},{2,4},{4,6},{6,8},{8,10},{10,12},{12,14},{14,16},{16,18},{18... | collective-permute-start | bytes 2162696 | tf_op jit(solution)/shard_map/ppermute | solution.py:100
  616.3 33.1 %collective-permute-start.13 = (bf16[2816,128]{1,0:T(8,128)(2,1)S(1)}, bf16[2816,128]{1,0:T(8,128)(2,1)S(1)}, u32[]{:S(2)}, u32[]{:S(2)}) collective-permute-start(bf16[2816,128]{1,0:T(8,128)(2,1)S(1)} %collective-permute-done.12), channel_id=1, source_target_pairs={{0,2},{2,4},{4,6},{6,8},{8,10},{10,12},{12,14},{14,16},{16,18},{18... | collective-permute-start | bytes 2162696 | tf_op jit(solution)/shard_map/ppermute | solution.py:100
  649.4 37.0 %copy-start.34 = (bf16[2816,128]{1,0:T(8,128)(2,1)}, bf16[2816,128]{1,0:T(8,128)(2,1)S(1)}, u32[]{:S(2)}) copy-start(bf16[2816,128]{1,0:T(8,128)(2,1)S(1)} %collective-permute-done.13) | copy-start | bytes 2162692
  649.4 37.0 %collective-permute-start.14 = (bf16[2816,128]{1,0:T(8,128)(2,1)S(1)}, bf16[2816,128]{1,0:T(8,128)(2,1)}, u32[]{:S(2)}, u32[]{:S(2)}) collective-permute-start(bf16[2816,128]{1,0:T(8,128)(2,1)S(1)} %collective-permute-done.13), channel_id=1, source_target_pairs={{0,2},{2,4},{4,6},{6,8},{8,10},{10,12},{12,14},{14,16},{16,18},{18... | collective-permute-start | bytes 2162696 | tf_op jit(solution)/shard_map/ppermute | solution.py:100
  686.4 15.1 %collective-permute-start.15 = (bf16[2816,128]{1,0:T(8,128)(2,1)}, bf16[2816,128]{1,0:T(8,128)(2,1)S(1)}, u32[]{:S(2)}, u32[]{:S(2)}) collective-permute-start(bf16[2816,128]{1,0:T(8,128)(2,1)} %collective-permute-done.14), channel_id=1, source_target_pairs={{0,2},{2,4},{4,6},{6,8},{8,10},{10,12},{12,14},{14,16},{16,18},{18... | collective-permute-start | bytes 2162696 | tf_op jit(solution)/shard_map/ppermute | solution.py:100
  686.5 18.1 %copy-start.35 = (bf16[2816,128]{1,0:T(8,128)(2,1)S(1)}, bf16[2816,128]{1,0:T(8,128)(2,1)}, u32[]{:S(2)}) copy-start(bf16[2816,128]{1,0:T(8,128)(2,1)} %copy-done.34) | copy-start | bytes 2162692
  689.3 16.3 %copy-start.33 = (bf16[2816,128]{1,0:T(8,128)(2,1)S(1)}, bf16[2816,128]{1,0:T(8,128)(2,1)}, u32[]{:S(2)}) copy-start(bf16[2816,128]{1,0:T(8,128)(2,1)} %copy-done.32) | copy-start | bytes 2162692
  689.3 17.3 %copy-start.31 = (bf16[2816,128]{1,0:T(8,128)(2,1)S(1)}, bf16[2816,128]{1,0:T(8,128)(2,1)}, u32[]{:S(2)}) copy-start(bf16[2816,128]{1,0:T(8,128)(2,1)} %copy-done.30) | copy-start | bytes 2162692
  702.5 5.1 copy-start.29
  704.6 3.9 copy-start.27
  705.6 3.9 copy-start.25
  706.5 3.9 copy-start.23
  708.5 3.9 copy-start.19
  709.5 4.0 copy-start.17
  744.4 25.8 %copy-start.53 = (f32[2048]{0:T(1024)S(1)}, f32[2048]{0:T(1024)}, u32[]{:S(2)}) copy-start(f32[2048]{0:T(1024)} %param.31) | copy-start | bytes 24580
  744.4 28.2 %copy-start.1 = (bf16[16,64,64]{2,1,0:T(8,128)(2,1)S(1)}, bf16[16,64,64]{2,1,0:T(8,128)(2,1)}, u32[]{:S(2)}) copy-start(bf16[16,64,64]{2,1,0:T(8,128)(2,1)} %param.22) | copy-start | bytes 393220
  (29 other events, 55.9 us)
Sparse Core Ops, SparseCore 0:
  236.1 19.3 all-reduce.33
  763.9 4.9 reduce-scatter.1
Sparse Core Ops, SparseCore 1:
  239.2 204.6 all-gather.4
  446.4 221.9 all-gather.6
